TPU v7x, 512 devices: a 4x2x32 block of a 4x8x32 slice. The times are simulated.
512 devices in a mesh: grp: 2 (over y), fs: 32 (over z), tp: 8 (over x, core).
Axes of the slice: x: 4, y: 2, z: 32, core: 2. Of those that a mesh axis runs over, the one named last changes fastest.
The devices are a block of a 4x8x32 slice.
Arguments:
- tokens: bfloat16 [12288, 2048], P(('grp', 'fs'), 'tp'), parts along dimension 0, may hold values from -40 to 40
- routes: int32 [12288, 8], P(('grp', 'fs')), parts along dimension 0, may hold values from 0 to 31, all different within a row; in each aligned block of 192 rows (0 to 191, 192 to 383, ...) at most 56 rows name the same one
- routing_weight: float32 [12288, 8], P(('grp', 'fs')), parts along dimension 0, may hold values from 0.1 to 0.6
- norm_gain_vector: float32 [2048], P('tp'), may hold values from 0.1 to 1.9
- expert_gate: float32 [32, 512, 2048], P(None, 'fs', 'tp'), may hold values from -0.125 to 0.125
- expert_up: float32 [32, 512, 2048], P(None, 'fs', 'tp'), may hold values from -0.125 to 0.125
- expert_down: float32 [32, 512, 2048], P(None, 'fs', 'tp'), may hold values from -0.25 to 0.25
- shared_gate: float32 [512, 2048], P('fs', 'tp'), may hold values from -0.125 to 0.125
- shared_up: float32 [512, 2048], P('fs', 'tp'), may hold values from -0.125 to 0.125
- shared_down: float32 [512, 2048], P('fs', 'tp'), may hold values from -0.25 to 0.25
Outputs:
- mixed: bfloat16 [12288, 2048], P(('grp', 'fs'), 'tp'), parts along dimension 0
- gate_served: bfloat16 [64, 512, 2048], P(('grp', 'fs'), None, 'tp'), parts along dimension 0
- up_served: bfloat16 [64, 512, 2048], P(('grp', 'fs'), None, 'tp'), parts along dimension 0
- down_served: bfloat16 [64, 512, 2048], P(('grp', 'fs'), None, 'tp'), parts along dimension 0
- shared_gate_served: bfloat16 [1024, 2048], P('grp', 'tp'), parts along dimension 0
- shared_up_served: bfloat16 [1024, 2048], P('grp', 'tp'), parts along dimension 0
- shared_down_served: bfloat16 [1024, 2048], P('grp', 'tp'), parts along dimension 0
There are 2 independent parts, one for each index of `grp`. A program takes and returns all parts, laid end to end along the dimension named above; an argument that names none is the same for every part. Nothing has to cross between parts.
Inputs may be any that keep to these rules, and one draw needn't show every extreme that they name: `routes`: each row names 8 different experts. In each aligned block of 192 rows no expert is named by more than 56 rows, and in some block an expert is named by exactly 56 rows.
All inputs are finite; a program needn't handle non-finite values.
Results may differ from a plain program's by a relative error of at most 0.022.
Values may be sent and summed in bfloat16 or wider, within the bound.
A program may use at most 64 MiB of HBM per device.

v0:
```python
import jax
import jax.numpy as jnp
from jax import lax
from jax.sharding import PartitionSpec as P

norm_eps = 1e-06


def sent_together(arrays, axis, split_dim, concat_dim, along):
    widths = [a.shape[along] for a in arrays]
    both = jnp.concatenate(arrays, axis=along)
    out = lax.all_to_all(both, axis, split_axis=split_dim, concat_axis=concat_dim, tiled=True)
    return tuple(jnp.split(out, [sum(widths[:k]) for k in range(1, len(widths))], axis=along))


def sent_together_2(arrays, axis, dim, along):
    both = jnp.concatenate(arrays, axis=along)
    out, at, outs = (lax.all_gather(both, axis, axis=dim, tiled=True), 0, [])
    for a in arrays:
        outs.append(lax.slice_in_dim(out, at, at + a.shape[along], axis=along))
        at += a.shape[along]
    return tuple(outs)


def in_one_piece(arrays, axis, dim, along):
    both = jnp.concatenate(arrays, axis=along)
    out, at, outs = (lax.psum_scatter(both, axis, scatter_dimension=dim, tiled=True), 0, [])
    for a in arrays:
        outs.append(lax.slice_in_dim(out, at, at + a.shape[along], axis=along))
        at += a.shape[along]
    return tuple(outs)


def dense_rows(rows, weight):
    return lax.dot_general(
        rows, weight, (((1,), (1,)), ((), ())), preferred_element_type=jnp.float32
    )


def per_device(
    tokens,
    routes,
    routing_weight,
    norm_gain_vector,
    expert_gate,
    expert_up,
    expert_down,
    shared_gate,
    shared_up,
    shared_down,
):
    tok_rows, portion_width = tokens.shape
    model_width = portion_width * lax.axis_size("tp")
    experts = expert_gate.shape[0]
    top_count = routes.shape[1]
    capacity = tok_rows * top_count * 7 // (6 * experts)
    gate_round = (expert_gate * norm_gain_vector[None, None, :]).astype(jnp.bfloat16)
    up_round = (expert_up * norm_gain_vector[None, None, :]).astype(jnp.bfloat16)
    down_round = expert_down.astype(jnp.bfloat16)
    gate_refreshed, up_new, down_new = sent_together(
        (gate_round, up_round, down_round), "fs", 0, 1, 2
    )
    shared_g, shared_u, shared_d = sent_together_2(
        (
            (shared_gate * norm_gain_vector[None, :]).astype(jnp.bfloat16),
            (shared_up * norm_gain_vector[None, :]).astype(jnp.bfloat16),
            shared_down.astype(jnp.bfloat16),
        ),
        "fs",
        0,
        1,
    )
    values = tokens.astype(jnp.float32)
    totals = lax.psum(jnp.sum(values * values, axis=1), "tp")
    normed = (values * lax.rsqrt(totals / model_width + norm_eps)[:, None]).astype(jnp.bfloat16)
    flat_expert = routes.reshape(-1)
    onehot = (flat_expert[:, None] == jnp.arange(experts, dtype=jnp.int32)[None, :]).astype(
        jnp.int32
    )
    earlier = jnp.cumsum(onehot, axis=0) - onehot
    slot_index = jnp.sum(earlier * onehot, axis=1)
    target = (flat_expert * capacity + slot_index).reshape(tok_rows, top_count)
    places = jnp.arange(experts * capacity, dtype=jnp.int32)
    placing = jnp.sum(
        (target[:, :, None] == places[None, None, :]).astype(jnp.int32), axis=1
    ).astype(jnp.bfloat16)
    outgoing = lax.dot_general(
        placing, normed, (((0,), (0,)), ((), ())), preferred_element_type=jnp.float32
    ).astype(jnp.bfloat16)
    incoming = lax.all_to_all(
        outgoing.reshape(experts, capacity, portion_width),
        "fs",
        split_axis=0,
        concat_axis=0,
        tiled=True,
    )
    arrived = incoming.reshape(experts * capacity, portion_width)
    partials = (
        dense_rows(arrived, gate_refreshed[0]).astype(jnp.bfloat16),
        dense_rows(arrived, up_new[0]).astype(jnp.bfloat16),
        dense_rows(normed, shared_g).astype(jnp.bfloat16),
        dense_rows(normed, shared_u).astype(jnp.bfloat16),
    )
    gate_part, up_part, sgate_part, sup_part = tuple(
        (
            part.astype(jnp.float32)
            for part in in_one_piece(
                (partials[0], partials[1], partials[2], partials[3]), "tp", 1, 0
            )
        )
    )
    hidden, shared_hidden = (
        lax.all_gather(
            (jax.nn.silu(gate_part) * up_part).astype(jnp.bfloat16), "tp", axis=1, tiled=True
        ),
        lax.all_gather(
            (jax.nn.silu(sgate_part) * sup_part).astype(jnp.bfloat16), "tp", axis=1, tiled=True
        ),
    )
    produced = jnp.dot(hidden, down_new[0], preferred_element_type=jnp.float32).astype(jnp.bfloat16)
    returned = lax.all_to_all(
        produced.reshape(experts, capacity, portion_width),
        "fs",
        split_axis=0,
        concat_axis=0,
        tiled=True,
    )
    picked = returned.reshape(experts * capacity, portion_width)[target]
    routed = jnp.sum(routing_weight[:, :, None] * picked.astype(jnp.float32), axis=1)
    shared_out = jnp.dot(shared_hidden, shared_d, preferred_element_type=jnp.float32)
    mixed = (routed + shared_out).astype(jnp.bfloat16)
    return (mixed, gate_refreshed, up_new, down_new, shared_g, shared_u, shared_d)


def solution(mesh):
    return jax.shard_map(
        per_device,
        mesh=mesh,
        in_specs=(
            P(("grp", "fs"), "tp"),
            P(("grp", "fs"), None),
            P(("grp", "fs"), None),
            P("tp"),
            P(None, "fs", "tp"),
            P(None, "fs", "tp"),
            P(None, "fs", "tp"),
            P("fs", "tp"),
            P("fs", "tp"),
            P("fs", "tp"),
        ),
        out_specs=(
            P(("grp", "fs"), "tp"),
            P(("grp", "fs"), None, "tp"),
            P(("grp", "fs"), None, "tp"),
            P(("grp", "fs"), None, "tp"),
            P("grp", "tp"),
            P("grp", "tp"),
            P("grp", "tp"),
        ),
        check_vma=False,
    )
```

profile of v0, /device:TPU:40, one launch (start us, length us, event | category | flops | bytes accessed | tf_op | source)
XLA Modules:
  0.0 523.9 jit_solution(1667189688354686824)
XLA Ops:
  7.2 1.1 convert_element_type.88
  8.3 1.3 multiply_convert_fusion.1
  9.6 1.0 pad_maximum_fusion.1
  10.6 45.8 %all-to-all-start.1 = ((bf16[32,16,768]{2,1,0:T(8,128)(2,1)}), bf16[32,16,768]{2,1,0:T(8,128)(2,1)S(1)}, u32[]{:S(2)}, u32[]{:S(2)}) async-start(bf16[32,16,768]{2,1,0:T(8,128)(2,1)} %pad_maximum_fusion.1), calls=%async_computation.1 | async-start | bytes 1572864 | tf_op jit(solution)/shard_map/all_to_all | solution.py:12
  56.7 9.1 %reduce-window.6 = s32[32,12,128]{2,1,0:T(8,128)S(1)} reduce-window(s32[32,12,128]{2,1,0:T(8,128)S(1)} %fusion.11, s32[]{:T(128)} %constant.6.clone.1), window={size=1x1x128 pad=0_0x0_0x127_0}, to_apply=%region_0.0 | reduce-window | flops 6242304 | bytes 393220 | tf_op jit(solution)/shard_map/reduce-window
  66.0 0.2 copy.47
  66.3 0.1 broadcast_add_fusion
  66.9 15.4 %psum.7 = f32[192]{0:T(256)S(1)} all-reduce(f32[192]{0:T(256)S(1)} %fusion.12), channel_id=1, replica_groups=mesh['grp'=2,'fs'=32,'tp'=8] {'tp'}, use_global_device_ids=true, to_apply=%region_5.6 | all-reduce | flops 192 | bytes 1536 | tf_op jit(solution)/shard_map/psum | solution.py:74
  82.4 5.0 convert_reduce_fusion
  87.4 1.5 convolution_convert_fusion.3
  88.9 53.8 %all-to-all-done.1 = bf16[32,16,768]{2,1,0:T(8,128)(2,1)S(1)} async-done(((bf16[32,16,768]{2,1,0:T(8,128)(2,1)}), bf16[32,16,768]{2,1,0:T(8,128)(2,1)S(1)}, u32[]{:S(2)}, u32[]{:S(2)}) %all-to-all-start.1) | async-done | bytes 786464 | tf_op jit(solution)/shard_map/all_to_all | solution.py:12
  142.7 4.8 all-to-all-start
  147.7 133.8 %all_gather.9 = bf16[512,768]{1,0:T(8,128)(2,1)S(1)} all-gather(bf16[16,768]{1,0:T(8,128)(2,1)S(1)} %pad_maximum_fusion.2), channel_id=1, replica_groups=mesh['grp'=2,'fs'=32,'tp'=8] {'fs'}, dimensions={0}, use_global_device_ids=true | all-gather | bytes 811008 | tf_op jit(solution)/shard_map/all_gather | solution.py:18
  281.6 0.2 convolution_convert_fusion.4
  281.9 0.9 convolution_convert_fusion.5
  282.9 0.7 convolution_convert_fusion
  283.6 0.7 convolution_convert_fusion.1
  284.3 0.2 copy-done.6
  284.6 2.1 pad_maximum_fusion
  286.6 6.3 %copy.56 = bf16[3968,512]{0,1:T(8,128)(2,1)} copy(bf16[3968,512]{1,0:T(8,128)(2,1)} %pad_maximum_fusion) | data formatting | bytes 8126464
  293.0 0.2 all-gather.2.cloned.1.call-start
  293.2 52.6 %reduce-scatter.4.cloned.1.call-done = bf16[64,3968]{1,0:T(8,128)(2,1)} async-done(((bf16[512,3968]{1,0:T(8,128)(2,1)}), bf16[64,3968]{1,0:T(8,128)(2,1)}) %reduce-scatter.4.cloned.1.call-update) | async-done | bytes 507920
  345.8 1.9 fusion.7
  347.8 40.5 %all-gather.2.cloned.1.call-done = bf16[1792,512]{0,1:T(8,128)(2,1)} async-done(((bf16[1792,64]{0,1:T(8,128)(2,1)}), bf16[1792,512]{0,1:T(8,128)(2,1)}) %all-gather.2.cloned.1.call-update) | async-done | bytes 1835024 | tf_op jit(solution)/shard_map/all_gather | solution.py:113
  388.2 3.1 convolution_convert_fusion.2
  391.4 23.6 %all-to-all-start.2 = ((bf16[32,56,256]{2,1,0:T(8,128)(2,1)}), bf16[32,56,256]{2,1,0:T(8,128)(2,1)S(1)}, u32[]{:S(2)}, u32[]{:S(2)}) async-start(bf16[32,56,256]{2,1,0:T(8,128)(2,1)} %bitcast.8), calls=%async_computation.2 | async-start | bytes 1835008 | tf_op jit(solution)/shard_map/all_to_all | solution.py:121
  415.4 0.9 fusion.21
  416.3 13.1 %all_gather.11 = bf16[192,512]{0,1:T(8,128)(2,1)S(1)} all-gather(bf16[192,64]{0,1:T(8,128)(2,1)S(1)} %fusion.21), channel_id=1, replica_groups=mesh['grp'=2,'fs'=32,'tp'=8] {'tp'}, dimensions={1}, use_global_device_ids=true | all-gather | bytes 221184 | tf_op jit(solution)/shard_map/all_gather | solution.py:116
  429.3 81.5 %all-to-all-done.2 = bf16[32,56,256]{2,1,0:T(8,128)(2,1)S(1)} async-done(((bf16[32,56,256]{2,1,0:T(8,128)(2,1)}), bf16[32,56,256]{2,1,0:T(8,128)(2,1)S(1)}, u32[]{:S(2)}, u32[]{:S(2)}) %all-to-all-start.2) | async-done | bytes 917536 | tf_op jit(solution)/shard_map/all_to_all | solution.py:121
  510.8 4.8 gather_fusion
  515.6 0.5 fusion
  516.1 0.9 fusion.1
  (54 shorter events, 1.8 us)
Async XLA Ops:
  9.6 46.8 %copy-start.8 = (s32[192,8]{0,1:T(8,128)S(1)}, s32[192,8]{0,1:T(8,128)}, u32[]{:S(2)}) copy-start(s32[192,8]{0,1:T(8,128)} %param.11) | copy-start | bytes 18436
  10.6 132.1 %all-to-all-start.1 = ((bf16[32,16,768]{2,1,0:T(8,128)(2,1)}), bf16[32,16,768]{2,1,0:T(8,128)(2,1)S(1)}, u32[]{:S(2)}, u32[]{:S(2)}) async-start(bf16[32,16,768]{2,1,0:T(8,128)(2,1)} %pad_maximum_fusion.1), calls=%async_computation.1 | async-start | bytes 1572864 | tf_op jit(solution)/shard_map/all_to_all | solution.py:12
  56.4 10.4 %copy-start = (bf16[192,256]{1,0:T(8,128)(2,1)S(1)}, bf16[192,256]{1,0:T(8,128)(2,1)}, u32[]{:S(2)}) copy-start(bf16[192,256]{1,0:T(8,128)(2,1)} %param.10) | copy-start | bytes 294916
  87.4 60.3 %copy-start.11 = (f32[16,256]{1,0:T(8,128)S(1)}, f32[16,256]{1,0:T(8,128)}, u32[]{:S(2)}) copy-start(f32[16,256]{1,0:T(8,128)} %param.19) | copy-start | bytes 49156
  87.4 60.3 %copy-start.9 = (f32[16,256]{1,0:T(8,128)S(1)}, f32[16,256]{1,0:T(8,128)}, u32[]{:S(2)}) copy-start(f32[16,256]{1,0:T(8,128)} %param.17) | copy-start | bytes 49156
  87.4 60.3 %copy-start.10 = (f32[16,256]{1,0:T(8,128)S(1)}, f32[16,256]{1,0:T(8,128)}, u32[]{:S(2)}) copy-start(f32[16,256]{1,0:T(8,128)} %param.18) | copy-start | bytes 49156
  87.4 60.3 %copy-start.13 = (f32[256]{0:T(256)S(1)}, f32[256]{0:T(256)}, u32[]{:S(2)}) copy-start(f32[256]{0:T(256)} %param.13) | copy-start | bytes 3076
  142.7 140.2 %all-to-all-start = ((bf16[32,56,256]{2,1,0:T(8,128)(2,1)}), bf16[32,56,256]{2,1,0:T(8,128)(2,1)S(1)}, u32[]{:S(2)}, u32[]{:S(2)}) async-start(bf16[32,56,256]{2,1,0:T(8,128)(2,1)} %bitcast.2), calls=%async_computation | async-start | bytes 1835008 | tf_op jit(solution)/shard_map/all_to_all | solution.py:90
  147.6 198.3 %reduce-scatter.4.cloned.1.call-start = ((), (), s32[]{:S(2)}) async-start(), calls=%async_computation.5 | async-start | bytes 4571136
  281.6 2.0 copy-start.4
  281.6 2.0 copy-start.5
  281.6 234.5 %copy-start.1 = (bf16[512,256]{1,0:T(8,128)(2,1)}, bf16[512,256]{1,0:T(8,128)(2,1)S(1)}, u32[]{:S(2)}) copy-start(bf16[512,256]{1,0:T(8,128)(2,1)S(1)} %get-tuple-element.9) | copy-start | bytes 786436
  282.9 1.4 copy-start.2
  282.9 1.4 copy-start.3
  282.9 105.3 %copy-start.7 = (bf16[1,512,256]{2,1,0:T(8,128)(2,1)}, bf16[1,512,256]{2,1,0:T(8,128)(2,1)S(1)}, u32[]{:S(2)}) copy-start(bf16[1,512,256]{2,1,0:T(8,128)(2,1)S(1)} %get-tuple-element.12) | copy-start | bytes 786436
  283.6 0.9 copy-start.6
  293.0 95.3 %all-gather.2.cloned.1.call-start = ((), (), s32[]{:S(2)}) async-start(), calls=%async_computation.4 | async-start | bytes 2064384 | tf_op jit(solution)/shard_map/all_gather | solution.py:113
  391.4 23.8 %copy-start.12 = (f32[192,8]{0,1:T(8,128)S(1)}, f32[192,8]{0,1:T(8,128)}, u32[]{:S(2)}) copy-start(f32[192,8]{0,1:T(8,128)} %param.12) | copy-start | bytes 18436
  391.4 119.5 %all-to-all-start.2 = ((bf16[32,56,256]{2,1,0:T(8,128)(2,1)}), bf16[32,56,256]{2,1,0:T(8,128)(2,1)S(1)}, u32[]{:S(2)}, u32[]{:S(2)}) async-start(bf16[32,56,256]{2,1,0:T(8,128)(2,1)} %bitcast.8), calls=%async_computation.2 | async-start | bytes 1835008 | tf_op jit(solution)/shard_map/all_to_all | solution.py:121
Sparse Core Ops, SparseCore 0:
  293.1 52.6 reduce-scatter.3
  348.0 40.2 all-gather.1
where the time goes:
time: 526 us; the launch traced here: 524 us
  waiting for transfers between devices  229 us (44%)
  blocking collectives  162 us (31%)
  starting transfers between devices  74.5 us (14%)
  other arithmetic  23.3 us (4%)
  between operations  14.5 us (3%)
  local copies, waits for them, and re-layouts  12.8 us (2%)
  matrix products  8.01 us (2%)
    all_gather x1, blocking collectives, sent_together_2(): out, at, outs = (lax.all_gather(both, axis, axis=dim, tiled=True), 0, [])  134 us
    all_to_all x1, waiting for transfers between devices, per_device(): lax.all_to_all(produced.reshape(experts, capacity, portion_width), 'fs',...  81.5 us
    all_to_all x1, waiting for transfers between devices, sent_together(): lax.all_to_all(both, axis, split_axis=split_dim, concat_axis=concat_dim,...  53.8 us
    unnamed x3, waiting for transfers between devices  52.7 us
    all_to_all x1, starting transfers between devices, sent_together(): lax.all_to_all(both, axis, split_axis=split_dim, concat_axis=concat_dim,...  45.8 us
    all_gather x1, waiting for transfers between devices, per_device(): lax.all_gather((jax.nn.silu(gate_part) * up_part).astype(jnp.bfloat16), '...  40.5 us
    all_to_all x1, starting transfers between devices, per_device(): lax.all_to_all(produced.reshape(experts, capacity, portion_width), 'fs',...  23.6 us
    psum x1, blocking collectives, per_device(): totals = lax.psum(jnp.sum(values * values, axis=1), 'tp')  15.4 us
  transfers between devices with their start and end apart: 5, of which 4 were waited for; matrix products, arithmetic and copies ran while one was open for 4% of the time, Pallas kernels for 0%

commit v1 on v0

v1 whole, which is shorter than its diff:
```python
import functools

import jax
import jax.numpy as jnp
from jax import lax
from jax.experimental import pallas as pl
from jax.experimental.pallas import tpu as pltpu
from jax.sharding import PartitionSpec as P

norm_eps = 1e-06
MESH = pl.DeviceIdType.MESH
GATHER_PIECES = 4
REDUCE_PIECES = 4
BF16 = jnp.bfloat16
F32 = jnp.float32


def contract(a, b, da, db):
    return lax.dot_general(a, b, (((da,), (db,)), ((), ())), preferred_element_type=F32)


def barrier_with(peers):
    barrier = pltpu.get_barrier_semaphore()
    for peer in peers:
        pl.semaphore_signal(barrier, inc=1, device_id=peer, device_id_type=MESH)
    pl.semaphore_wait(barrier, len(peers))


def gather_kernel(n, pieces, block, out, send_sem, recv_sem, own_sem):
    me = lax.axis_index("fs")
    right, left = lax.rem(me + 1, n), lax.rem(me + n - 1, n)
    rows = block.shape[0] // pieces
    reach = (n // 2, n - 1 - n // 2)

    def copy(way, step, piece, first=False):
        whose = lax.rem(me + n - step, n) if way == 0 else lax.rem(me + step, n)
        part = pl.ds(piece * rows, rows)
        target = out.at[whose, part, :]
        return pltpu.make_async_remote_copy(
            src_ref=block.at[part, :] if first else target,
            dst_ref=target,
            send_sem=send_sem.at[way, step, piece],
            recv_sem=recv_sem.at[way, step, piece],
            device_id={"fs": right if way == 0 else left},
            device_id_type=MESH,
        )

    def arrived(way, step, piece):
        whose = lax.rem(me + 2 * n - step - 1, n) if way == 0 else lax.rem(me + step + 1, n)
        target = out.at[whose, pl.ds(piece * rows, rows), :]
        pltpu.make_async_remote_copy(
            src_ref=target,
            dst_ref=target,
            send_sem=send_sem.at[way, step, piece],
            recv_sem=recv_sem.at[way, step, piece],
            device_id={"fs": left if way == 0 else right},
            device_id_type=MESH,
        ).wait_recv()

    own = pltpu.make_async_copy(block, out.at[me], own_sem)
    own.start()
    barrier_with([{"fs": left}, {"fs": right}])
    for piece in range(pieces):
        for way in range(2):
            if reach[way] > 0:
                copy(way, 0, piece, True).start()

    def step_of(ways):
        def body(step, carry):
            for piece in range(pieces):
                for way in ways:
                    arrived(way, step - 1, piece)
                    copy(way, step, piece).start()
            return carry

        return body

    lax.fori_loop(1, reach[1], step_of((0, 1)), 0)
    lax.fori_loop(max(reach[1], 1), reach[0], step_of((0,)), 0)
    for piece in range(pieces):
        for way in range(2):
            if reach[way] > 0:
                arrived(way, reach[way] - 1, piece)
    own.wait()
    for way in range(2):
        for piece in range(pieces):
            copy(way, 0, piece, True).wait_send()

        def sent(step, carry, way=way):
            for piece in range(pieces):
                copy(way, step, piece).wait_send()
            return carry

        lax.fori_loop(1, reach[way], sent, 0)


def ring_gather(n, block):
    reach = n // 2
    return pl.pallas_call(
        functools.partial(gather_kernel, n, GATHER_PIECES),
        out_shape=jax.ShapeDtypeStruct((n,) + block.shape, block.dtype),
        in_specs=[pl.BlockSpec(memory_space=pltpu.VMEM)],
        out_specs=pl.BlockSpec(memory_space=pltpu.VMEM),
        scratch_shapes=[
            pltpu.SemaphoreType.DMA((2, reach, GATHER_PIECES)),
            pltpu.SemaphoreType.DMA((2, reach, GATHER_PIECES)),
            pltpu.SemaphoreType.DMA,
        ],
        compiler_params=pltpu.CompilerParams(collective_id=0, has_side_effects=True),
        cost_estimate=pl.CostEstimate(flops=10**9, bytes_accessed=10**7, transcendentals=0),
        name="ring_gather",
    )(block)


def layer_kernel(
    n,
    tp,
    shared_rows,
    pieces,
    rows_ref,
    gate_ref,
    up_ref,
    down_ref,
    sgate_ref,
    sup_ref,
    sdown_ref,
    place_ref,
    out_ref,
    psend,
    precv,
    total,
    passed,
    direct,
    final,
    own_total,
    hidden,
    combined,
    shared_out,
    ring,
    pair_send,
    pair_recv,
    sum_send,
    sum_recv,
    hid_send,
    hid_recv,
    ring_send,
    ring_recv,
):
    me = lax.axis_index("fs")
    t = lax.axis_index("tp")
    right, left = lax.rem(me + 1, n), lax.rem(me + n - 1, n)
    chips = tp // 2
    x, core = t // 2, lax.rem(t, 2)

    def chip(offset):
        return lax.rem(x + offset + chips, chips)

    mate = 2 * x + 1 - core
    ahead, behind = 2 * chip(1) + core, 2 * chip(-1) + core
    share_rows, width = rows_ref.shape[1], 2 * gate_ref.shape[0]
    ff = gate_ref.shape[0]
    routed = share_rows - (share_rows - n // tp * place_ref.shape[1])
    half = share_rows // 2

    barrier_with(
        [{"fs": left}, {"fs": right}, {"tp": mate}, {"tp": ahead}, {"tp": behind}]
    )

    def partial_sums(share, put):
        put(0, routed, 0, contract(rows_ref[share, 0:routed, :], gate_ref[...], 1, 1))
        put(0, routed, ff, contract(rows_ref[share, 0:routed, :], up_ref[...], 1, 1))
        put(routed, share_rows, 0, contract(rows_ref[share, routed:, :], sgate_ref[...], 1, 1))
        put(routed, share_rows, ff, contract(rows_ref[share, routed:, :], sup_ref[...], 1, 1))

    def remote(src, dst, send_sem, recv_sem, peer):
        return pltpu.make_async_remote_copy(
            src_ref=src,
            dst_ref=dst,
            send_sem=send_sem,
            recv_sem=recv_sem,
            device_id={"tp": peer},
            device_id_type=MESH,
        )

    def pair_copy(r):
        return remote(psend.at[r], precv.at[r], pair_send.at[r], pair_recv.at[r], mate)

    for r in (2, 1, 3, 0):

        def put(a, b, c, value, r=r):
            psend[r, a:b, c : c + ff] = value.astype(BF16)

        partial_sums(2 * chip(r) + 1 - core, put)
        pair_copy(r).start()

    top, low = pl.ds(0, half), pl.ds(half, half)
    pass_top = remote(total.at[2, top, :], passed.at[0], sum_send.at[0], sum_recv.at[0], ahead)
    pass_low = remote(total.at[2, low, :], passed.at[1], sum_send.at[1], sum_recv.at[1], behind)
    direct_low = remote(total.at[1, low, :], direct.at[1], sum_send.at[2], sum_recv.at[2], ahead)
    direct_top = remote(total.at[3, top, :], direct.at[0], sum_send.at[3], sum_recv.at[3], behind)
    final_top = remote(total.at[1, top, :], final.at[0], sum_send.at[4], sum_recv.at[4], ahead)
    final_low = remote(total.at[3, low, :], final.at[1], sum_send.at[5], sum_recv.at[5], behind)
    for r in (2, 1, 3, 0):
        pair_copy(r).wait_recv()

        def put(a, b, c, value, r=r):
            value = value + precv[r, a:b, c : c + ff].astype(F32)
            if r == 0:
                own_total[a:b, c : c + ff] = value
            else:
                total[r, a:b, c : c + ff] = value.astype(BF16)

        partial_sums(2 * chip(r) + core, put)
        if r == 2:
            pass_top.start()
            pass_low.start()
        if r == 1:
            direct_low.start()
        if r == 3:
            direct_top.start()

    def add_rows(slot, start, source):
        total[slot, start : start + half, :] = (
            total[slot, start : start + half, :].astype(F32) + source.astype(F32)
        ).astype(BF16)

    pass_top.wait_recv()
    add_rows(1, 0, passed[0])
    final_top.start()
    pass_low.wait_recv()
    add_rows(3, half, passed[1])
    final_low.start()
    direct_low.wait_recv()
    direct_top.wait_recv()
    final_top.wait_recv()
    final_low.wait_recv()

    for k in range(2):
        span = slice(k * half, (k + 1) * half)

        def summed(c, k=k, span=span):
            cols = slice(c, c + ff)
            return (
                own_total[span, cols]
                + direct[k, :, cols].astype(F32)
                + final[k, :, cols].astype(F32)
            )

        g = summed(0)
        hidden[t, span, :] = (g / (1.0 + jnp.exp(-g)) * summed(ff)).astype(BF16)

    def hid(slot, span, k, peer):
        ref = hidden.at[slot, span, :]
        return remote(ref, ref, hid_send.at[k], hid_recv.at[k], peer)

    whole = pl.ds(0, share_rows)
    mine, opposite = t, 2 * chip(2) + core
    hid(mine, whole, 1, ahead).start()
    hid(mine, whole, 2, behind).start()
    hid(mine, whole, 0, mate).start()
    hid(behind, whole, 1, behind).wait_recv()
    hid(behind, top, 3, ahead).start()
    hid(behind, whole, 5, mate).start()
    hid(ahead, whole, 2, ahead).wait_recv()
    hid(ahead, low, 4, behind).start()
    hid(ahead, whole, 6, mate).start()
    hid(opposite, top, 3, behind).wait_recv()
    hid(opposite, top, 7, mate).start()
    hid(opposite, low, 4, ahead).wait_recv()
    hid(opposite, low, 8, mate).start()

    def other(slot):
        return 2 * (slot // 2) + 1 - lax.rem(slot, 2)

    hid(other(mine), whole, 0, mate).wait_recv()
    hid(other(behind), whole, 5, mate).wait_recv()
    hid(other(ahead), whole, 6, mate).wait_recv()
    hid(other(opposite), top, 7, mate).wait_recv()
    hid(other(opposite), low, 8, mate).wait_recv()

    per_share = n // tp
    capacity = place_ref.shape[1]

    def down_of(share, carry):
        produced = contract(hidden[share, 0:routed, :], down_ref[...], 1, 0)
        for q in range(per_share):
            piece = produced[q * capacity : (q + 1) * capacity, :].astype(BF16)
            block = share * per_share + q
            combined[block] = contract(place_ref[block], piece, 0, 0).astype(BF16)
        extra = contract(hidden[share, routed:, :], sdown_ref[...], 1, 0)
        start = pl.multiple_of(share * shared_rows, 8)
        shared_out[pl.ds(start, shared_rows), :] = extra[0:shared_rows, :]
        return carry

    lax.fori_loop(0, tp, down_of, 0)

    reach = (n // 2, n - 1 - n // 2)
    size = combined.shape[1] // pieces

    def spot(way, step):
        ahead_by = reach[way] - step
        return lax.rem(me + ahead_by, n) if way == 0 else lax.rem(me + n - ahead_by, n)

    def ring_copy(way, step, piece, first=False):
        part = pl.ds(piece * size, size)
        if first:
            src = combined.at[spot(way, step), part, :]
        else:
            src = ring.at[way, step - 1, part, :]
        return pltpu.make_async_remote_copy(
            src_ref=src,
            dst_ref=ring.at[way, step, part, :],
            send_sem=ring_send.at[way, step, piece],
            recv_sem=ring_recv.at[way, step, piece],
            device_id={"fs": right if way == 0 else left},
            device_id_type=MESH,
        )

    for piece in range(pieces):
        for way in range(2):
            ring_copy(way, 0, piece, True).start()

    def ring_step(ways):
        def body(step, carry):
            for piece in range(pieces):
                for way in ways:
                    ring_copy(way, step - 1, piece, True).wait_recv()
                    part = pl.ds(piece * size, size)
                    ring[way, step - 1, part, :] = (
                        ring[way, step - 1, part, :].astype(F32)
                        + combined[spot(way, step), part, :].astype(F32)
                    ).astype(BF16)
                    ring_copy(way, step, piece).start()
            return carry

        return body

    lax.fori_loop(1, reach[1], ring_step((0, 1)), 0)
    lax.fori_loop(max(reach[1], 1), reach[0], ring_step((0,)), 0)
    for piece in range(pieces):
        part = slice(piece * size, (piece + 1) * size)
        for way in range(2):
            ring_copy(way, reach[way] - 1, piece, True).wait_recv()
        out_ref[part, :] = (
            ring[0, reach[0] - 1, part, :].astype(F32)
            + ring[1, reach[1] - 1, part, :].astype(F32)
            + combined[me, part, :].astype(F32)
            + shared_out[part, :]
        ).astype(BF16)

    for r in range(4):
        pair_copy(r).wait_send()
    for c in (pass_top, pass_low, direct_low, direct_top, final_top, final_low):
        c.wait_send()
    for span, ks in ((whole, (0, 1, 2, 5, 6)), (top, (3, 7)), (low, (4, 8))):
        for k in ks:
            hid(mine, span, k, mate).wait_send()
    for way in range(2):
        for piece in range(pieces):
            ring_copy(way, 0, piece, True).wait_send()

        def sent(step, carry, way=way):
            for piece in range(pieces):
                ring_copy(way, step, piece).wait_send()
            return carry

        lax.fori_loop(1, reach[way], sent, 0)


def run_layer(n, tp, tok_rows, rows, weights, place):
    shares, share_rows, width = rows.shape
    ff = weights[0].shape[0]
    chips, half = tp // 2, share_rows // 2
    reach = n // 2
    dma = pltpu.SemaphoreType.DMA
    return pl.pallas_call(
        functools.partial(layer_kernel, n, tp, tok_rows // tp, REDUCE_PIECES),
        out_shape=jax.ShapeDtypeStruct((tok_rows, width), BF16),
        in_specs=[pl.BlockSpec(memory_space=pltpu.VMEM)] * 8,
        out_specs=pl.BlockSpec(memory_space=pltpu.VMEM),
        scratch_shapes=[
            pltpu.VMEM((chips, share_rows, 2 * ff), BF16),
            pltpu.VMEM((chips, share_rows, 2 * ff), BF16),
            pltpu.VMEM((chips, share_rows, 2 * ff), BF16),
            pltpu.VMEM((2, half, 2 * ff), BF16),
            pltpu.VMEM((2, half, 2 * ff), BF16),
            pltpu.VMEM((2, half, 2 * ff), BF16),
            pltpu.VMEM((share_rows, 2 * ff), F32),
            pltpu.VMEM((tp, share_rows, ff), BF16),
            pltpu.VMEM((n, tok_rows, width), BF16),
            pltpu.VMEM((tok_rows, width), F32),
            pltpu.VMEM((2, reach, tok_rows, width), BF16),
            dma((chips,)),
            dma((chips,)),
            dma((6,)),
            dma((6,)),
            dma((9,)),
            dma((9,)),
            dma((2, reach, REDUCE_PIECES)),
            dma((2, reach, REDUCE_PIECES)),
        ],
        compiler_params=pltpu.CompilerParams(collective_id=1, has_side_effects=True),
        cost_estimate=pl.CostEstimate(flops=2 * 10**9, bytes_accessed=10**7, transcendentals=0),
        name="expert_layer",
    )(rows, *weights, place)


def per_device(
    n,
    tp,
    tokens,
    routes,
    routing_weight,
    norm_gain_vector,
    expert_gate,
    expert_up,
    expert_down,
    shared_gate,
    shared_up,
    shared_down,
):
    tok_rows, width = tokens.shape
    experts = expert_gate.shape[0]
    top_count = routes.shape[1]
    capacity = tok_rows * top_count * 7 // (6 * experts)
    gain = norm_gain_vector
    both = jnp.concatenate(
        [
            (expert_gate * gain[None, None, :]).astype(BF16),
            (expert_up * gain[None, None, :]).astype(BF16),
            expert_down.astype(BF16),
        ],
        axis=2,
    )
    moved = lax.all_to_all(both, "fs", split_axis=0, concat_axis=1, tiled=True)
    gate_new, up_new, down_new = jnp.split(moved, 3, axis=2)

    values = tokens.astype(F32)
    totals = lax.psum(jnp.sum(values * values, axis=1), "tp")
    normed = (values * lax.rsqrt(totals / (width * tp) + norm_eps)[:, None]).astype(BF16)

    def as_lanes(a):
        return jnp.pad(a.T.astype(BF16), ((0, 0), (0, width - tok_rows)))

    block = jnp.concatenate(
        [
            normed,
            (shared_gate * gain[None, :]).astype(BF16),
            (shared_up * gain[None, :]).astype(BF16),
            shared_down.astype(BF16),
            as_lanes(routes),
            as_lanes(routing_weight),
        ],
        axis=0,
    )
    got = ring_gather(n, block)
    unit = shared_gate.shape[0]
    at = tok_rows
    shared = []
    for _ in range(3):
        shared.append(got[:, at : at + unit, :].reshape(n * unit, width))
        at += unit
    sgate, sup, sdown = shared
    chosen_by = got[:, at : at + top_count, :tok_rows]
    weight_of = got[:, at + top_count : at + 2 * top_count, :tok_rows]
    mine = chosen_by.astype(F32) == lax.axis_index("fs").astype(F32)
    weights = jnp.sum(jnp.where(mine, weight_of.astype(F32), 0.0), axis=1)
    named = jnp.any(mine, axis=1)
    index = jnp.arange(tok_rows, dtype=jnp.int32)
    before = (index[:, None] < index[None, :]).astype(BF16)
    rank = jnp.dot(named.astype(BF16), before, preferred_element_type=F32)
    slot = jnp.where(named, rank, -1.0)
    hit = slot[:, None, :] == jnp.arange(capacity, dtype=jnp.int32).astype(F32)[None, :, None]
    place = jnp.where(hit, weights[:, None, :], 0.0).astype(BF16)
    picked = jnp.einsum(
        "bsj,bjd->bsd", hit.astype(BF16), got[:, :tok_rows, :], preferred_element_type=F32
    ).astype(BF16)
    per_share = n // tp * capacity
    shared_rows = tok_rows // tp
    rows = jnp.concatenate(
        [
            picked.reshape(tp, per_share, width),
            normed.reshape(tp, shared_rows, width),
            jnp.zeros((tp, -(per_share + shared_rows) % 32, width), BF16),
        ],
        axis=1,
    )
    mixed = run_layer(
        n,
        tp,
        tok_rows,
        rows,
        (gate_new[0], up_new[0], down_new[0], sgate, sup, sdown),
        place,
    )
    return (mixed, gate_new, up_new, down_new, sgate, sup, sdown)


def solution(mesh):
    return jax.shard_map(
        functools.partial(per_device, mesh.shape["fs"], mesh.shape["tp"]),
        mesh=mesh,
        in_specs=(
            P(("grp", "fs"), "tp"),
            P(("grp", "fs"), None),
            P(("grp", "fs"), None),
            P("tp"),
            P(None, "fs", "tp"),
            P(None, "fs", "tp"),
            P(None, "fs", "tp"),
            P("fs", "tp"),
            P("fs", "tp"),
            P("fs", "tp"),
        ),
        out_specs=(
            P(("grp", "fs"), "tp"),
            P(("grp", "fs"), None, "tp"),
            P(("grp", "fs"), None, "tp"),
            P(("grp", "fs"), None, "tp"),
            P("grp", "tp"),
            P("grp", "tp"),
            P("grp", "tp"),
        ),
        check_vma=False,
    )
```

time: 526 us -> 298 us (0.57)
  waiting for transfers between devices: 229 us -> 0.01 us
  Pallas kernels: 0 us -> 220 us
  blocking collectives: 162 us -> 14.8 us
  starting transfers between devices: 74.5 us -> 45.8 us
  other arithmetic: 23.3 us -> 8.21 us
  between operations: 14.5 us -> 0.85 us
  local copies, waits for them, and re-layouts: 12.8 us -> 5.23 us
    pallas_call x0 -> x2, Pallas kernels: none -> 220 us  [the longest x1 118 us: ring_gather(): pl.pallas_call(functools.partial(gather_kernel, n, GATHER_PIECES), out_sh...]
    all_gather x2 -> x0, blocking collectives: 147 us -> none  [the longest x1 134 us: sent_together_2(): out, at, outs = (lax.all_gather(both, axis, axis=dim, tiled=True), 0, [])]
    all_to_all x3 -> x1, waiting for transfers between devices: 135 us -> 0.01 us  [per_device(): moved = lax.all_to_all(both, 'fs', split_axis=0, concat_axis=1, tiled=True)]
    unnamed x3 -> x0, waiting for transfers between devices: 52.7 us -> none
    all_gather x1 -> x0, waiting for transfers between devices: 40.5 us -> none  [per_device(): lax.all_gather((jax.nn.silu(gate_part) * up_part).astype(jnp.bfloat16), '...]
    all_to_all x3 -> x1, starting transfers between devices: 74.2 us -> 45.8 us  [per_device(): moved = lax.all_to_all(both, 'fs', split_axis=0, concat_axis=1, tiled=True)]
    another operation x3 -> x0, other arithmetic: 9.24 us -> none
  transfers between devices with their start and end apart: 5 -> 1, of which waited for: 4 -> 0; matrix products, arithmetic and copies ran while one was open for 4% -> 3% of each run, Pallas kernels for 0% -> 40%
where the time goes in v1:
time: 298 us; the launch traced here: 297 us
  Pallas kernels  220 us (74%)
  starting transfers between devices  45.8 us (15%)
  blocking collectives  14.8 us (5%)
  other arithmetic  8.21 us (3%)
  local copies, waits for them, and re-layouts  5.23 us (2%)
    pallas_call x1, Pallas kernels, ring_gather(): pl.pallas_call(functools.partial(gather_kernel, n, GATHER_PIECES), out_sh...  118 us
    pallas_call x1, Pallas kernels, run_layer(): pl.pallas_call(functools.partial(layer_kernel, n, tp, tok_rows // tp, RED...  102 us
    all_to_all x1, starting transfers between devices, per_device(): moved = lax.all_to_all(both, 'fs', split_axis=0, concat_axis=1, tiled=True)  45.8 us
    psum x1, blocking collectives, per_device(): totals = lax.psum(jnp.sum(values * values, axis=1), 'tp')  14.8 us
  transfers between devices with their start and end apart: 1, of which 0 were waited for; matrix products, arithmetic and copies ran while one was open for 3% of the time, Pallas kernels for 40%

profile of v1, /device:TPU:40, one launch (start us, length us, event | category | flops | bytes accessed | tf_op | source)
XLA Modules:
  0.0 297.4 jit_solution(3323725759403325959)
XLA Ops:
  0.6 1.1 convert_element_type.79
  1.7 0.0 copy-start.1
  1.7 0.0 copy-start.6
  1.7 1.4 multiply_convert_fusion.1
  3.1 0.0 copy-start.3
  3.1 0.0 copy-start.5
  3.1 0.0 copy-start.4
  3.2 0.0 copy-start.2
  3.2 0.0 copy-start.7
  3.2 1.0 pad_maximum_fusion
  4.1 45.8 %all-to-all-start = ((bf16[32,16,768]{2,1,0:T(8,128)(2,1)}), bf16[32,16,768]{2,1,0:T(8,128)(2,1)S(1)}, u32[]{:S(2)}, u32[]{:S(2)}) async-start(bf16[32,16,768]{2,1,0:T(8,128)(2,1)} %pad_maximum_fusion), calls=%async_computation | async-start | bytes 1572864 | tf_op jit(solution)/shard_map/all_to_all | solution.py:435
  49.9 0.1 pad.14.clone
  50.0 0.0 copy-done.1
  50.0 0.1 fusion.11
  50.1 14.8 %psum.7 = f32[192]{0:T(256)S(1)} all-reduce(f32[192]{0:T(256)S(1)} %fusion.11), channel_id=1, replica_groups=mesh['grp'=2,'fs'=32,'tp'=8] {'tp'}, use_global_device_ids=true, to_apply=%region_1.0 | all-reduce | flops 192 | bytes 1536 | tf_op jit(solution)/shard_map/psum | solution.py:439
  65.0 0.0 copy-done.6
  65.0 0.1 constant_dynamic-update-slice_fusion.5
  65.1 0.0 copy-done.4
  65.2 0.0 copy-start
  65.2 0.6 copy-done
  65.9 118.0 %ring_gather.1 = bf16[32,256,256]{2,1,0:T(8,128)(2,1)} custom-call(bf16[256,256]{1,0:T(8,128)(2,1)} %copy-done), custom_call_target="tpu_custom_call" | custom-call | flops 1000000000 | bytes 10000000 | tf_op jit(solution)/shard_map/ring_gather/pallas_call | solution.py:99
  183.9 1.0 fusion.13
  184.9 1.1 select_reduce_fusion
  186.0 0.1 convolution_select_fusion
  186.1 1.2 fusion.3.place_ref
  187.4 2.0 fusion.15
  189.4 2.6 fusion.4
  192.0 1.2 maximum_maximum_fusion.rows_ref
  193.2 0.0 all-to-all-done
  193.2 0.9 fusion.16
  194.1 101.7 %expert_layer.1 = bf16[192,256]{1,0:T(8,128)(2,1)} custom-call(bf16[8,256,256]{2,1,0:T(8,128)(2,1)} %maximum_maximum_fusion.rows_ref, bf16[512,256]{1,0:T(8,128)(2,1)} %bitcast.25, bf16[512,256]{1,0:T(8,128)(2,1)} %bitcast.24, bf16[512,256]{1,0:T(8,128)(2,1)} %bitcast.23, bf16[512,256]{1,0:T(8,128)(2,1)} %bitcast.21, bf16[512,256]{1,0:T(8,128)(2,1)} %bitcast.19, ...), custom_call_target="tpu_custom_call" | custom-call | flops 2000000000 | bytes 10000000 | tf_op jit(solution)/shard_map/expert_layer/pallas_call | solution.py:376
  295.8 1.5 copy.23
  (14 shorter events, 0.1 us)
Async XLA Ops:
  1.7 48.3 %copy-start.1 = (bf16[192,256]{1,0:T(8,128)(2,1)S(1)}, bf16[192,256]{1,0:T(8,128)(2,1)}, u32[]{:S(2)}) copy-start(bf16[192,256]{1,0:T(8,128)(2,1)} %param.10) | copy-start | bytes 294916
  1.7 63.3 %copy-start.6 = (s32[192,8]{0,1:T(8,128)S(1)}, s32[192,8]{0,1:T(8,128)}, u32[]{:S(2)}) copy-start(s32[192,8]{0,1:T(8,128)} %param.11) | copy-start | bytes 18436
  3.1 62.0 %copy-start.3 = (f32[16,256]{1,0:T(8,128)S(1)}, f32[16,256]{1,0:T(8,128)}, u32[]{:S(2)}) copy-start(f32[16,256]{1,0:T(8,128)} %param.17) | copy-start | bytes 49156
  3.1 62.0 %copy-start.5 = (f32[256]{0:T(256)S(1)}, f32[256]{0:T(256)}, u32[]{:S(2)}) copy-start(f32[256]{0:T(256)} %param.13) | copy-start | bytes 3076
  3.1 62.0 %copy-start.4 = (f32[16,256]{1,0:T(8,128)S(1)}, f32[16,256]{1,0:T(8,128)}, u32[]{:S(2)}) copy-start(f32[16,256]{1,0:T(8,128)} %param.18) | copy-start | bytes 49156
  3.2 62.0 %copy-start.2 = (f32[16,256]{1,0:T(8,128)S(1)}, f32[16,256]{1,0:T(8,128)}, u32[]{:S(2)}) copy-start(f32[16,256]{1,0:T(8,128)} %param.19) | copy-start | bytes 49156
  3.2 62.0 %copy-start.7 = (f32[192,8]{0,1:T(8,128)S(1)}, f32[192,8]{0,1:T(8,128)}, u32[]{:S(2)}) copy-start(f32[192,8]{0,1:T(8,128)} %param.12) | copy-start | bytes 18436
  4.1 189.1 %all-to-all-start = ((bf16[32,16,768]{2,1,0:T(8,128)(2,1)}), bf16[32,16,768]{2,1,0:T(8,128)(2,1)S(1)}, u32[]{:S(2)}, u32[]{:S(2)}) async-start(bf16[32,16,768]{2,1,0:T(8,128)(2,1)} %pad_maximum_fusion), calls=%async_computation | async-start | bytes 1572864 | tf_op jit(solution)/shard_map/all_to_all | solution.py:435
  65.2 0.7 copy-start

commit v2 on v1

--- a/solution.py
+++ b/solution.py
@@ -26,8 +26,12 @@
     pl.semaphore_wait(barrier, len(peers))
 
 
-def gather_kernel(n, pieces, block, out, send_sem, recv_sem, own_sem):
+def gather_kernel(
+    n, groups, pieces, block, held, out, full, send_sem, recv_sem, own_sem, y_send, y_recv, y_own
+):
     me = lax.axis_index("fs")
+    group = lax.axis_index("grp")
+    cols, share = full.shape[0], held.shape[1]
     right, left = lax.rem(me + 1, n), lax.rem(me + n - 1, n)
     rows = block.shape[0] // pieces
     reach = (n // 2, n - 1 - n // 2)
@@ -59,11 +63,41 @@
 
     own = pltpu.make_async_copy(block, out.at[me], own_sem)
     own.start()
-    barrier_with([{"fs": left}, {"fs": right}])
+    others = [lax.rem(group + j, groups) for j in range(1, groups)]
+    barrier_with([{"fs": left}, {"fs": right}] + [{"grp": g} for g in others])
     for piece in range(pieces):
         for way in range(2):
             if reach[way] > 0:
                 copy(way, 0, piece, True).start()
+
+    def handed(j, i, sender):
+        piece = sender * share + i
+        peer = lax.rem(group + j, groups)
+        return piece < cols, lambda: pltpu.make_async_remote_copy(
+            src_ref=held.at[:, i],
+            dst_ref=full.at[jnp.minimum(piece, cols - 1)],
+            send_sem=y_send.at[j - 1, i],
+            recv_sem=y_recv.at[j - 1, i],
+            device_id={"grp": peer},
+            device_id_type=MESH,
+        )
+
+    def kept(i):
+        piece = group * share + i
+        return piece < cols, lambda: pltpu.make_async_copy(
+            held.at[:, i], full.at[jnp.minimum(piece, cols - 1)], y_own.at[i]
+        )
+
+    def when_all(pairs, act):
+        for used, make in pairs:
+
+            @pl.when(used)
+            def _(make=make):
+                act(make())
+
+    order = [(j, i) for j in range(1, groups) for i in range(share)]
+    when_all([handed(j, i, group) for j, i in order], lambda c: c.start())
+    when_all([kept(i) for i in range(share)], lambda c: c.start())
 
     def step_of(ways):
         def body(step, carry):
@@ -82,6 +116,10 @@
             if reach[way] > 0:
                 arrived(way, reach[way] - 1, piece)
     own.wait()
+    senders = [(j, i, lax.rem(group + groups - j, groups)) for j, i in order]
+    when_all([handed(j, i, sender) for j, i, sender in senders], lambda c: c.wait_recv())
+    when_all([kept(i) for i in range(share)], lambda c: c.wait())
+    when_all([handed(j, i, group) for j, i in order], lambda c: c.wait_send())
     for way in range(2):
         for piece in range(pieces):
             copy(way, 0, piece, True).wait_send()
@@ -94,22 +132,30 @@
         lax.fori_loop(1, reach[way], sent, 0)
 
 
-def ring_gather(n, block):
+def ring_gather(n, groups, cols, block, held):
     reach = n // 2
+    share = held.shape[1]
+    vmem = pl.BlockSpec(memory_space=pltpu.VMEM)
     return pl.pallas_call(
-        functools.partial(gather_kernel, n, GATHER_PIECES),
-        out_shape=jax.ShapeDtypeStruct((n,) + block.shape, block.dtype),
-        in_specs=[pl.BlockSpec(memory_space=pltpu.VMEM)],
-        out_specs=pl.BlockSpec(memory_space=pltpu.VMEM),
+        functools.partial(gather_kernel, n, groups, GATHER_PIECES),
+        out_shape=(
+            jax.ShapeDtypeStruct((n,) + block.shape, block.dtype),
+            jax.ShapeDtypeStruct((cols, n) + held.shape[2:], held.dtype),
+        ),
+        in_specs=[vmem, vmem],
+        out_specs=(vmem, vmem),
         scratch_shapes=[
             pltpu.SemaphoreType.DMA((2, reach, GATHER_PIECES)),
             pltpu.SemaphoreType.DMA((2, reach, GATHER_PIECES)),
             pltpu.SemaphoreType.DMA,
+            pltpu.SemaphoreType.DMA((max(groups - 1, 1), share)),
+            pltpu.SemaphoreType.DMA((max(groups - 1, 1), share)),
+            pltpu.SemaphoreType.DMA((share,)),
         ],
         compiler_params=pltpu.CompilerParams(collective_id=0, has_side_effects=True),
         cost_estimate=pl.CostEstimate(flops=10**9, bytes_accessed=10**7, transcendentals=0),
         name="ring_gather",
-    )(block)
+    )(block, held)
 
 
 def layer_kernel(
@@ -406,6 +452,7 @@
 
 
 def per_device(
+    groups,
     n,
     tp,
     tokens,
@@ -424,16 +471,20 @@
     top_count = routes.shape[1]
     capacity = tok_rows * top_count * 7 // (6 * experts)
     gain = norm_gain_vector
-    both = jnp.concatenate(
-        [
-            (expert_gate * gain[None, None, :]).astype(BF16),
-            (expert_up * gain[None, None, :]).astype(BF16),
-            expert_down.astype(BF16),
-        ],
-        axis=2,
-    )
-    moved = lax.all_to_all(both, "fs", split_axis=0, concat_axis=1, tiled=True)
-    gate_new, up_new, down_new = jnp.split(moved, 3, axis=2)
+    lanes = 128
+    halves = []
+    for whole in (
+        (expert_gate * gain[None, None, :]).astype(BF16),
+        (expert_up * gain[None, None, :]).astype(BF16),
+        expert_down.astype(BF16),
+    ):
+        halves += [whole[:, :, c : c + lanes] for c in range(0, width, lanes)]
+    share = -(-len(halves) // groups)
+    first = lax.rem(lax.axis_index("grp") * share, len(halves))
+    mine = lax.dynamic_slice_in_dim(
+        jnp.stack(halves + halves[: share - 1], axis=1), first, share, axis=1
+    )
+    held = lax.all_to_all(mine, "fs", split_axis=0, concat_axis=0, tiled=True)
 
     values = tokens.astype(F32)
     totals = lax.psum(jnp.sum(values * values, axis=1), "tp")
@@ -453,7 +504,11 @@
         ],
         axis=0,
     )
-    got = ring_gather(n, block)
+    got, full = ring_gather(n, groups, len(halves), block, held)
+    full = full.reshape(3, width // lanes, -1, lanes)
+    gate_new, up_new, down_new = (
+        jnp.concatenate([full[k, c] for c in range(width // lanes)], axis=1) for k in range(3)
+    )
     unit = shared_gate.shape[0]
     at = tok_rows
     shared = []
@@ -490,15 +545,15 @@
         tp,
         tok_rows,
         rows,
-        (gate_new[0], up_new[0], down_new[0], sgate, sup, sdown),
+        (gate_new, up_new, down_new, sgate, sup, sdown),
         place,
     )
-    return (mixed, gate_new, up_new, down_new, sgate, sup, sdown)
+    return (mixed, gate_new[None], up_new[None], down_new[None], sgate, sup, sdown)
 
 
 def solution(mesh):
     return jax.shard_map(
-        functools.partial(per_device, mesh.shape["fs"], mesh.shape["tp"]),
+        functools.partial(per_device, mesh.shape["grp"], mesh.shape["fs"], mesh.shape["tp"]),
         mesh=mesh,
         in_specs=(
             P(("grp", "fs"), "tp"),

time: 298 us -> 281 us (0.943)
  Pallas kernels: 220 us -> 163 us
  waiting for transfers between devices: 0.01 us -> 37.8 us
    pallas_call x1, Pallas kernels: 118 us -> 62.2 us  [ring_gather(): pl.pallas_call(functools.partial(gather_kernel, n, groups, GATHER_PIECES)...]
    all_to_all x1, waiting for transfers between devices: 0.01 us -> 37.8 us  [per_device(): held = lax.all_to_all(mine, 'fs', split_axis=0, concat_axis=0, tiled=True)]
  transfers between devices with their start and end apart: 1 -> 1, of which waited for: 0 -> 1; matrix products, arithmetic and copies ran while one was open for 3% -> 0% of each run, Pallas kernels for 40% -> 0%
where the time goes in v2:
time: 281 us; the launch traced here: 279 us
  Pallas kernels  163 us (58%)
  starting transfers between devices  45.8 us (16%)
  waiting for transfers between devices  37.8 us (13%)
  blocking collectives  14.8 us (5%)
  other arithmetic  9.16 us (3%)
  local copies, waits for them, and re-layouts  5.56 us (2%)
    pallas_call x1, Pallas kernels, run_layer(): pl.pallas_call(functools.partial(layer_kernel, n, tp, tok_rows // tp, RED...  100 us
    pallas_call x1, Pallas kernels, ring_gather(): pl.pallas_call(functools.partial(gather_kernel, n, groups, GATHER_PIECES)...  62.2 us
    all_to_all x1, starting transfers between devices, per_device(): held = lax.all_to_all(mine, 'fs', split_axis=0, concat_axis=0, tiled=True)  45.8 us
    all_to_all x1, waiting for transfers between devices, per_device(): held = lax.all_to_all(mine, 'fs', split_axis=0, concat_axis=0, tiled=True)  37.8 us
    psum x1, blocking collectives, per_device(): totals = lax.psum(jnp.sum(values * values, axis=1), 'tp')  14.8 us
  transfers between devices with their start and end apart: 1, of which 1 were waited for; matrix products, arithmetic and copies ran while one was open for 0% of the time, Pallas kernels for 0%

profile of v2, /device:TPU:40, one launch (start us, length us, event | category | flops | bytes accessed | tf_op | source)
XLA Modules:
  0.0 279.4 jit_solution(15585639747149008762)
XLA Ops:
  0.6 1.1 convert_element_type.75
  1.7 1.3 multiply_convert_fusion
  3.1 0.0 copy-start.2
  3.1 0.0 copy-start.8
  3.1 0.0 copy-start.5
  3.1 0.0 copy-start.7
  3.1 0.0 copy-start.6
  3.1 0.0 copy-start.4
  3.1 0.0 copy-start.9
  3.5 0.8 constant_dynamic-slice_fusion
  4.3 45.8 %all-to-all-start = ((bf16[32,3,16,128]{3,2,1,0:T(8,128)(2,1)}), bf16[32,3,16,128]{3,2,1,0:T(8,128)(2,1)S(1)}, u32[]{:S(2)}, u32[]{:S(2)}) async-start(bf16[32,3,16,128]{3,2,1,0:T(8,128)(2,1)} %constant_dynamic-slice_fusion), calls=%async_computation | async-start | bytes 786432 | tf_op jit(solution)/shard_map/all_to_all | solution.py:487
  50.1 0.1 pad.17.clone
  50.1 0.1 fusion.11
  50.3 14.8 %psum.7 = f32[192]{0:T(256)S(1)} all-reduce(f32[192]{0:T(256)S(1)} %fusion.11), channel_id=1, replica_groups=mesh['grp'=2,'fs'=32,'tp'=8] {'tp'}, use_global_device_ids=true, to_apply=%region_1.0 | all-reduce | flops 192 | bytes 1536 | tf_op jit(solution)/shard_map/psum | solution.py:490
  65.1 0.0 copy-done.8
  65.1 0.1 constant_dynamic-update-slice_fusion.5
  65.3 0.0 copy-start.3
  65.4 37.8 %all-to-all-done.held = bf16[32,3,16,128]{3,2,1,0:T(8,128)(2,1)S(1)} async-done(((bf16[32,3,16,128]{3,2,1,0:T(8,128)(2,1)}), bf16[32,3,16,128]{3,2,1,0:T(8,128)(2,1)S(1)}, u32[]{:S(2)}, u32[]{:S(2)}) %all-to-all-start) | async-done | bytes 393248 | tf_op jit(solution)/shard_map/all_to_all | solution.py:487
  103.2 0.8 copy-done.1
  104.0 62.2 %ring_gather.1 = (bf16[32,256,256]{2,1,0:T(8,128)(2,1)}, bf16[6,32,16,128]{3,2,1,0:T(8,128)(2,1)}) custom-call(bf16[256,256]{1,0:T(8,128)(2,1)} %copy-done.3, bf16[32,3,16,128]{3,2,1,0:T(8,128)(2,1)} %copy-done.1), custom_call_target="tpu_custom_call" | custom-call | flops 1000000000 | bytes 10000000 | tf_op jit(solution)/shard_map/ring_gather/pallas_call | solution.py:139
  166.2 1.1 fusion.21
  167.3 1.1 select_reduce_fusion
  168.4 2.0 fusion.26
  170.4 0.1 slice_bitcast_fusion.1
  170.5 0.1 convolution_select_fusion
  170.6 2.6 fusion.4
  173.2 1.3 fusion.3.place_ref
  174.5 0.8 fusion.24
  175.4 1.2 maximum_maximum_fusion.rows_ref
  176.6 1.0 fusion.22
  177.6 100.3 %expert_layer.1 = bf16[192,256]{1,0:T(8,128)(2,1)} custom-call(bf16[8,256,256]{2,1,0:T(8,128)(2,1)} %maximum_maximum_fusion.rows_ref, bf16[512,256]{1,0:T(8,128)(2,1)} %get-tuple-element.27.gate_ref, bf16[512,256]{1,0:T(8,128)(2,1)} %get-tuple-element.30.up_ref, bf16[512,256]{1,0:T(8,128)(2,1)} %get-tuple-element.23.down_ref, bf16[512,256]{1,0:T(8,128)(2,1)} %bitcast.73, ...), custom_call_target="tpu_custom_call" | custom-call | flops 2000000000 | bytes 10000000 | tf_op jit(solution)/shard_map/expert_layer/pallas_call | solution.py:422
  277.9 1.5 copy.35
  (28 shorter events, 0.3 us)
Async XLA Ops:
  3.1 47.1 %copy-start.2 = (bf16[192,256]{1,0:T(8,128)(2,1)S(1)}, bf16[192,256]{1,0:T(8,128)(2,1)}, u32[]{:S(2)}) copy-start(bf16[192,256]{1,0:T(8,128)(2,1)} %param.10) | copy-start | bytes 294916
  3.1 62.0 %copy-start.8 = (s32[192,8]{0,1:T(8,128)S(1)}, s32[192,8]{0,1:T(8,128)}, u32[]{:S(2)}) copy-start(s32[192,8]{0,1:T(8,128)} %param.11) | copy-start | bytes 18436
  3.1 62.1 %copy-start.5 = (f32[16,256]{1,0:T(8,128)S(1)}, f32[16,256]{1,0:T(8,128)}, u32[]{:S(2)}) copy-start(f32[16,256]{1,0:T(8,128)} %param.17) | copy-start | bytes 49156
  3.1 62.1 %copy-start.7 = (f32[256]{0:T(256)S(1)}, f32[256]{0:T(256)}, u32[]{:S(2)}) copy-start(f32[256]{0:T(256)} %param.13) | copy-start | bytes 3076
  3.1 62.1 %copy-start.6 = (f32[16,256]{1,0:T(8,128)S(1)}, f32[16,256]{1,0:T(8,128)}, u32[]{:S(2)}) copy-start(f32[16,256]{1,0:T(8,128)} %param.18) | copy-start | bytes 49156
  3.1 62.1 %copy-start.4 = (f32[16,256]{1,0:T(8,128)S(1)}, f32[16,256]{1,0:T(8,128)}, u32[]{:S(2)}) copy-start(f32[16,256]{1,0:T(8,128)} %param.19) | copy-start | bytes 49156
  3.1 62.2 %copy-start.9 = (f32[192,8]{0,1:T(8,128)S(1)}, f32[192,8]{0,1:T(8,128)}, u32[]{:S(2)}) copy-start(f32[192,8]{0,1:T(8,128)} %param.12) | copy-start | bytes 18436
  4.3 98.9 %all-to-all-start = ((bf16[32,3,16,128]{3,2,1,0:T(8,128)(2,1)}), bf16[32,3,16,128]{3,2,1,0:T(8,128)(2,1)S(1)}, u32[]{:S(2)}, u32[]{:S(2)}) async-start(bf16[32,3,16,128]{3,2,1,0:T(8,128)(2,1)} %constant_dynamic-slice_fusion), calls=%async_computation | async-start | bytes 786432 | tf_op jit(solution)/shard_map/all_to_all | solution.py:487
  65.3 37.9 %copy-start.3 = (bf16[256,256]{1,0:T(8,128)(2,1)}, bf16[256,256]{1,0:T(8,128)(2,1)S(1)}, u32[]{:S(2)}) copy-start(bf16[256,256]{1,0:T(8,128)(2,1)S(1)} %constant_dynamic-update-slice_fusion.block) | copy-start | bytes 393220
  103.2 0.8 copy-start.1
  166.2 4.2 %copy-start = (bf16[6,32,16,128]{3,2,1,0:T(8,128)(2,1)S(1)}, bf16[6,32,16,128]{3,2,1,0:T(8,128)(2,1)}, u32[]{:S(2)}) copy-start(bf16[6,32,16,128]{3,2,1,0:T(8,128)(2,1)} %get-tuple-element.10) | copy-start | bytes 2359300
